TPU v7x, 32 devices: a whole 2x2x4 slice. The times are simulated.
32 devices in a mesh: sp: 8 (over z, x), dp: 4 (over y, core).
Axes of the slice: x: 2, y: 2, z: 4, core: 2. Of those that a mesh axis runs over, the one named last changes fastest.
Arguments:
- resid: bfloat16 [4, 1024, 2048], P('dp', 'sp'), may hold values from -6 to 6
- queries: bfloat16 [4, 1024, 2048], P('dp', 'sp'), may hold values from -7 to 7
- keys: bfloat16 [4, 1024, 2048], P('dp', 'sp'), may hold values from -7 to 7
- values: bfloat16 [4, 1024, 2048], P('dp', 'sp'), may hold values from -6 to 6
- forget_cache: float32 [4, 32, 1024], P('dp', 'sp'), may hold values from -131 to 0, as said below
- query_gain: float32 [64], replicated, may hold values from 0.5 to 8
- key_gain: float32 [64], replicated, may hold values from 0.5 to 8
- out_weight: bfloat16 [2048, 2048], P(None, 'dp'), may hold values from -0.125 to 0.125
- norm_gain: float32 [2048], replicated, may hold values from 0.1 to 1.9
- routes: int32 [4, 1024, 2], P('dp', 'sp'), may hold values from 0 to 31, all different within a row; in each aligned block of 128 rows (0 to 127, 128 to 255, ..., all dimensions but the last counted through in order) at most 16 rows name the same one
- group_weight: float32 [4, 1024], P('dp', 'sp'), may hold values from 0.2 to 1
- inner_share: float32 [4, 1024, 2], P('dp', 'sp'), may hold values from 0.1 to 1
- expert_gate: bfloat16 [32, 2048, 1024], P(('sp', 'dp')), may hold values from -0.125 to 0.125
- expert_up: bfloat16 [32, 2048, 1024], P(('sp', 'dp')), may hold values from -0.125 to 0.125
- expert_down: bfloat16 [32, 1024, 2048], P(('sp', 'dp')), may hold values from -0.1875 to 0.1875
Outputs:
- layer_out: bfloat16 [4, 1024, 2048], P('dp', 'sp')
Inputs may be any that keep to these rules, and one draw needn't show every extreme that they name: `routes`: each row names 2 different experts; the rows of one device name one expert at most 16 times, a bound that some block reaches. `forget_cache`: along positions each head's values never rise.
All inputs are finite; a program needn't handle non-finite values.
Results may differ from a plain program's by a relative error of at most 0.0095.
The roundings to bfloat16 on the way count: a program that leaves them out, or rounds other values in their place, can miss the bound.
Values may be sent and summed in bfloat16 or wider, within the bound.
No kernel may reach another device: no remote copies, remote signals or barrier semaphores. Data moves between devices by JAX's collectives and lax.ppermute only.
A program may use at most 128 MiB of HBM per device.

v0:
```python
import functools

import jax
import jax.numpy as jnp
from jax import lax
from jax.experimental import pallas as pl
from jax.experimental.pallas import tpu as pltpu
from jax.sharding import PartitionSpec as P

EPS = 1e-06


def norm_rows(inputs, gain):
    floats = inputs.astype(jnp.float32)
    scaled = floats * lax.rsqrt(jnp.mean(floats * floats, axis=-1, keepdims=True) + EPS)
    return (scaled * gain).astype(jnp.bfloat16)


LANES = 128
ROWS = 256


def pack_kernel(query_ref, key_ref, value_ref, *out_refs):
    lanes = out_refs[0].shape[2]
    tokens = query_ref.shape[0]
    chunks = len(out_refs)
    for peer in range(out_refs[0].shape[0]):
        for chunk in range(chunks):
            start = (peer * chunks + chunk) * lanes
            for place, ref in enumerate((query_ref, key_ref, value_ref)):
                out_refs[chunk][peer, place * tokens : (place + 1) * tokens, :] = ref[
                    :, start : start + lanes
                ]


def pack_heads(queries, keys, values, peers, chunks, lanes):
    tokens = queries.shape[0]
    shape = jax.ShapeDtypeStruct((peers, 3 * tokens, lanes), queries.dtype)
    return pl.pallas_call(
        pack_kernel,
        out_shape=[shape] * chunks,
        name="pack_heads",
        cost_estimate=pl.CostEstimate(
            flops=queries.size, bytes_accessed=12 * queries.size, transcendentals=0
        ),
    )(queries, keys, values)


def attend_kernel(
    tokens, head_size, rows, qkv_ref, gains_ref, level_ref, column_ref, out_ref, q_ref, k_ref, v_ref
):
    peers, _, lanes = qkv_ref.shape
    length = peers * tokens
    packed = lanes // head_size
    scale = head_size ** (-0.5)
    lane_head = lax.broadcasted_iota(jnp.int32, (1, lanes), 1) // head_size
    same = (
        lax.broadcasted_iota(jnp.int32, (lanes, lanes), 0) // head_size
        == lax.broadcasted_iota(jnp.int32, (lanes, lanes), 1) // head_size
    ).astype(jnp.bfloat16)

    def normed(part, gain):
        floats = part.astype(jnp.float32)
        squares = floats * floats
        high = squares.astype(jnp.bfloat16)
        low = (squares - high.astype(jnp.float32)).astype(jnp.bfloat16)
        total = jnp.dot(high, same, preferred_element_type=jnp.float32) + jnp.dot(
            low, same, preferred_element_type=jnp.float32
        )
        return (floats * lax.rsqrt(total * (1.0 / head_size) + EPS) * gain).astype(jnp.bfloat16)

    for peer in range(peers):
        place = slice(peer * tokens, (peer + 1) * tokens)
        query = normed(qkv_ref[peer, :tokens, :], gains_ref[0:1, :])
        key = normed(qkv_ref[peer, tokens : 2 * tokens, :], gains_ref[1:2, :])
        value = qkv_ref[peer, 2 * tokens :, :]
        k_ref[place, :] = key
        for head in range(packed):
            own = lane_head == head
            q_ref[head, place, :] = jnp.where(own, query, jnp.zeros_like(query))
            v_ref[head, place, :] = jnp.where(own, value, jnp.ones_like(value))

    inside = lax.broadcasted_iota(jnp.int32, (rows, rows), 1) <= lax.broadcasted_iota(
        jnp.int32, (rows, rows), 0
    )
    contract = (((1,), (1,)), ((), ()))
    for start in range(0, length, rows):
        stop = start + rows
        outs = []
        for head in range(packed):
            query = q_ref[head, start:stop, :]
            row_level = column_ref[start:stop, head : head + 1]
            last = lax.dot_general(
                query, k_ref[start:stop, :], contract, preferred_element_type=jnp.float32
            )
            last = jnp.where(inside, last * scale - level_ref[head : head + 1, start:stop], -jnp.inf)
            highest = jnp.max(last, axis=1, keepdims=True)
            if start:
                early = lax.dot_general(
                    query, k_ref[:start, :], contract, preferred_element_type=jnp.float32
                )
                early = early * scale - level_ref[head : head + 1, :start]
                highest = jnp.maximum(highest, jnp.max(early, axis=1, keepdims=True))
            shift = row_level - (highest + row_level)
            out = jnp.dot(
                jnp.exp(last + shift).astype(jnp.bfloat16),
                v_ref[head, start:stop, :],
                preferred_element_type=jnp.float32,
            )
            if start:
                out = out + jnp.dot(
                    jnp.exp(early + shift).astype(jnp.bfloat16),
                    v_ref[head, :start, :],
                    preferred_element_type=jnp.float32,
                )
            outs.append(out)
        numerator, sums = outs[0], outs[1]
        for head in range(1, packed):
            numerator = jnp.where(lane_head == head, outs[head], numerator)
            sums = jnp.where(lane_head == head, outs[head - 1], sums)
        sums = pltpu.roll(sums, head_size, 1) if packed == 2 else sum_lanes(outs, lane_head, head_size)
        out_ref[start:stop, :] = (numerator / sums).astype(out_ref.dtype)


def sum_lanes(outs, lane_head, head_size):
    packed = len(outs)
    total = jnp.zeros_like(outs[0])
    for head in range(packed):
        other = (head + 1) % packed * head_size
        total = jnp.where(lane_head == head, outs[head][:, other : other + 1], total)
    return total


def attend(qkv, gains, level, level_columns, tokens, head_size):
    peers, _, lanes = qkv.shape
    length = peers * tokens
    packed = lanes // head_size
    rows = ROWS if length % ROWS == 0 else tokens
    return pl.pallas_call(
        functools.partial(attend_kernel, tokens, head_size, rows),
        out_shape=jax.ShapeDtypeStruct((length, lanes), jnp.bfloat16),
        scratch_shapes=[
            pltpu.VMEM((packed, length, lanes), jnp.bfloat16),
            pltpu.VMEM((length, lanes), jnp.bfloat16),
            pltpu.VMEM((packed, length, lanes), jnp.bfloat16),
        ],
        compiler_params=pltpu.CompilerParams(vmem_limit_bytes=32 * 1024 * 1024),
        name="attend",
        cost_estimate=pl.CostEstimate(
            flops=4 * packed * length * length * lanes,
            bytes_accessed=8 * length * lanes,
            transcendentals=packed * length * length,
        ),
    )(qkv, gains, level, level_columns)


def gather_shards(shard, axis):
    size = lax.axis_size(axis)
    held = [shard]
    stride = size // 2
    offsets = [0]
    while stride:
        pairs = [(index, index ^ stride) for index in range(size)]
        held = held + [lax.ppermute(part, axis, pairs) for part in held]
        offsets = offsets + [offset ^ stride for offset in offsets]
        stride //= 2
    ordered = [None] * size
    for part, offset in zip(held, offsets):
        ordered[offset] = part
    return ordered


def order_pieces(pieces, axis):
    size = lax.axis_size(axis)
    own = lax.axis_index(axis)
    stride = 1
    while stride < size:
        flip = (own & stride) != 0
        pieces = [
            jnp.where(flip, pieces[index ^ stride], pieces[index]) for index in range(size)
        ]
        stride *= 2
    return pieces


def shards(
    resid,
    queries,
    keys,
    values,
    forget_cache,
    query_gain,
    key_gain,
    out_weight,
    norm_gain,
    routes,
    group_weight,
    inner_share,
    expert_gate,
    expert_up,
    expert_down,
):
    dp_size = lax.axis_size("dp")
    sp_size = lax.axis_size("sp")
    tokens = queries.shape[1]
    head_size = query_gain.shape[0]
    local_heads = forget_cache.shape[1]
    local_width = local_heads * head_size
    lanes = LANES if local_width % LANES == 0 else local_width
    chunks = local_width // lanes
    packed = lanes // head_size
    sends = pack_heads(queries[0], keys[0], values[0], sp_size, chunks, lanes)
    arrived_qkv = [
        lax.all_to_all(send, "sp", split_axis=0, concat_axis=0, tiled=True) for send in sends
    ]
    weight_shards = gather_shards(out_weight, "dp")
    gains = jnp.stack([jnp.tile(query_gain, packed), jnp.tile(key_gain, packed)])
    level = forget_cache[0]
    level_columns = level.T
    returned_heads = []
    for chunk in range(chunks):
        first = chunk * packed
        block = attend(
            arrived_qkv[chunk],
            gains,
            level[first : first + packed],
            level_columns[:, first : first + packed],
            tokens,
            head_size,
        )
        returned_heads.append(
            lax.all_to_all(
                block.reshape(sp_size, tokens, lanes),
                "sp",
                split_axis=0,
                concat_axis=0,
                tiled=True,
            )
        )
    token_attn = (
        jnp.stack(returned_heads, axis=1)
        .transpose(2, 0, 1, 3)
        .reshape(tokens, sp_size * local_width)
    )
    pieces = [
        jnp.dot(token_attn, shard, preferred_element_type=jnp.float32) for shard in weight_shards
    ]
    pieces = order_pieces(pieces, "dp")
    projected = jnp.concatenate(pieces, axis=1)
    mid = (resid[0].astype(jnp.float32) + projected).astype(jnp.bfloat16)
    normed = norm_rows(mid, norm_gain)
    width = normed.shape[1]
    tok_count = normed.shape[0]
    top_count = routes.shape[2]
    experts = lax.axis_size("sp") * lax.axis_size("dp")
    capacity = 2 * tok_count * top_count // experts
    expert_ids = routes[0].reshape(-1)
    expert_onehot = (expert_ids[:, None] == jnp.arange(experts, dtype=jnp.int32)[None, :]).astype(
        jnp.int32
    )
    earlier = jnp.cumsum(expert_onehot, axis=0) - expert_onehot
    slot_rank = jnp.sum(earlier * expert_onehot, axis=1)
    slot_index = (expert_ids * capacity + slot_rank).reshape(tok_count, top_count)
    slot_range = jnp.arange(experts * capacity, dtype=jnp.int32)
    dispatch = jnp.any(slot_range[:, None, None] == slot_index[None, :, :], axis=2).astype(
        jnp.bfloat16
    )
    send = jnp.dot(dispatch, normed, preferred_element_type=jnp.float32).astype(jnp.bfloat16)
    arrived = lax.all_to_all(
        send.reshape(experts, capacity, width),
        ("sp", "dp"),
        split_axis=0,
        concat_axis=0,
        tiled=True,
    )
    flat_rows = arrived.reshape(-1, width)
    gate = jnp.dot(flat_rows, expert_gate[0], preferred_element_type=jnp.float32)
    upper = jnp.dot(flat_rows, expert_up[0], preferred_element_type=jnp.float32)
    hidden = (jax.nn.silu(gate) * upper).astype(jnp.bfloat16)
    result = jnp.dot(hidden, expert_down[0], preferred_element_type=jnp.float32).astype(
        jnp.bfloat16
    )
    returned = lax.all_to_all(
        result.reshape(arrived.shape), ("sp", "dp"), split_axis=0, concat_axis=0, tiled=True
    )
    returned = returned.reshape(experts * capacity, width)
    shares = inner_share[0]
    weights = group_weight[0][:, None] * shares / jnp.sum(shares, axis=-1, keepdims=True)
    mixed = jnp.zeros((tok_count, width), jnp.float32)
    for route in range(top_count):
        select = (slot_range[None, :] == slot_index[:, route : route + 1]).astype(jnp.bfloat16)
        picked = jnp.dot(select, returned, preferred_element_type=jnp.float32)
        mixed = mixed + weights[:, route : route + 1] * picked
    layer_out = (mid.astype(jnp.float32) + mixed).astype(jnp.bfloat16)
    return layer_out.reshape(1, tok_count, width)


def solution(mesh):
    return jax.shard_map(
        shards,
        mesh=mesh,
        in_specs=(
            P("dp", "sp", None),
            P("dp", "sp", None),
            P("dp", "sp", None),
            P("dp", "sp", None),
            P("dp", "sp", None),
            P(),
            P(),
            P(None, "dp"),
            P(),
            P("dp", "sp", None),
            P("dp", "sp"),
            P("dp", "sp", None),
            P(("sp", "dp"), None, None),
            P(("sp", "dp"), None, None),
            P(("sp", "dp"), None, None),
        ),
        out_specs=P("dp", "sp", None),
        check_vma=False,
    )
```

profile of v0, /device:TPU:0, one launch (start us, length us, event | category | flops | bytes accessed | tf_op | source)
XLA Modules:
  0.0 220.8 jit_solution(11694701795129023600)
XLA Ops:
  0.0 2.8 %pack_heads.1 = (bf16[8,384,128]{2,1,0:T(8,128)(2,1)}, bf16[8,384,128]{2,1,0:T(8,128)(2,1)}) custom-call(bf16[128,2048]{1,0:T(8,128)(2,1)} %bitcast.102, bf16[128,2048]{1,0:T(8,128)(2,1)} %bitcast.103, bf16[128,2048]{1,0:T(8,128)(2,1)} %bitcast.104), custom_call_target="tpu_custom_call" | custom-call | flops 262144 | bytes 3145728 | tf_op jit(solution)/shard_map/pack_heads/pallas_call | solution.py:39
  2.8 7.3 %all-to-all-start = ((bf16[8,384,128]{2,1,0:T(8,128)(2,1)}), bf16[8,384,128]{2,1,0:T(8,128)(2,1)S(1)}, u32[]{:S(2)}, u32[]{:S(2)}) async-start(bf16[8,384,128]{2,1,0:T(8,128)(2,1)} %get-tuple-element.7), calls=%async_computation | async-start | bytes 1572864 | tf_op jit(solution)/shard_map/all_to_all | solution.py:214
  10.0 1.5 collective-permute-start
  11.6 18.7 %all-to-all-done.qkv_ref = bf16[8,384,128]{2,1,0:T(8,128)(2,1)S(1)} async-done(((bf16[8,384,128]{2,1,0:T(8,128)(2,1)}), bf16[8,384,128]{2,1,0:T(8,128)(2,1)S(1)}, u32[]{:S(2)}, u32[]{:S(2)}) %all-to-all-start) | async-done | bytes 786464 | tf_op jit(solution)/shard_map/all_to_all | solution.py:214
  30.2 3.7 %all-to-all-start.2 = ((bf16[8,384,128]{2,1,0:T(8,128)(2,1)}), bf16[8,384,128]{2,1,0:T(8,128)(2,1)S(1)}, u32[]{:S(2)}, u32[]{:S(2)}) async-start(bf16[8,384,128]{2,1,0:T(8,128)(2,1)} %get-tuple-element.8), calls=%async_computation.2 | async-start | bytes 1572864 | tf_op jit(solution)/shard_map/all_to_all | solution.py:214
  34.0 0.2 copy.32
  34.2 0.2 fusion.34
  34.6 22.8 %collective-permute-done = bf16[2048,512]{1,0:T(8,128)(2,1)} collective-permute-done((bf16[2048,512]{1,0:T(8,128)(2,1)}, bf16[2048,512]{1,0:T(8,128)(2,1)}, u32[]{:S(2)}, u32[]{:S(2)}) %collective-permute-start) | collective-permute-done | bytes 2097184 | tf_op jit(solution)/shard_map/ppermute | solution.py:164
  57.5 4.5 %attend.2 = bf16[1024,128]{1,0:T(8,128)(2,1)S(1)} custom-call(bf16[8,384,128]{2,1,0:T(8,128)(2,1)S(1)} %all-to-all-done.qkv_ref, f32[2,128]{1,0:T(2,128)S(1)} %pad_maximum_fusion.1.gains_ref, f32[2,1024]{1,0:T(2,128)S(1)} %get-tuple-element.19.level_ref, f32[1024,2]{1,0:T(8,128)S(1)} %get-tuple-element.17.column_ref), custom_call_target="tpu_custom_call" | custom-call | flops 1073741824 | bytes 1048576 | tf_op jit(solution)/shard_map/attend/pallas_call | solution.py:139
  62.0 0.9 copy.33
  62.9 5.7 %all-to-all-start.1 = ((bf16[8,128,128]{1,2,0:T(8,128)(2,1)}), bf16[8,128,128]{1,2,0:T(8,128)(2,1)S(1)}, u32[]{:S(2)}, u32[]{:S(2)}) async-start(bf16[8,128,128]{1,2,0:T(8,128)(2,1)} %copy.33), calls=%async_computation.1 | async-start | bytes 524288 | tf_op jit(solution)/shard_map/all_to_all | solution.py:232
  69.0 0.6 reduce-window.6
  69.6 0.2 slice_reduce_fusion.2
  69.8 4.5 %attend.3 = bf16[1024,128]{1,0:T(8,128)(2,1)S(1)} custom-call(bf16[8,384,128]{2,1,0:T(8,128)(2,1)S(1)} %all-to-all-done.2.qkv_ref, f32[2,128]{1,0:T(2,128)S(1)} %pad_maximum_fusion.1.gains_ref, f32[2,1024]{1,0:T(2,128)S(1)} %get-tuple-element.20.level_ref, f32[1024,2]{1,0:T(8,128)S(1)} %get-tuple-element.18.column_ref), custom_call_target="tpu_custom_call" | custom-call | flops 1073741824 | bytes 1048576 | tf_op jit(solution)/shard_map/attend/pallas_call | solution.py:139
  74.3 0.9 copy.34
  75.2 3.0 %all-to-all-done.1 = bf16[8,128,128]{1,2,0:T(8,128)(2,1)S(1)} async-done(((bf16[8,128,128]{1,2,0:T(8,128)(2,1)}), bf16[8,128,128]{1,2,0:T(8,128)(2,1)S(1)}, u32[]{:S(2)}, u32[]{:S(2)}) %all-to-all-start.1) | async-done | bytes 262176 | tf_op jit(solution)/shard_map/all_to_all | solution.py:232
  78.2 3.6 %all-to-all-start.3 = ((bf16[8,128,128]{1,2,0:T(8,128)(2,1)}), bf16[8,128,128]{1,2,0:T(8,128)(2,1)S(1)}, u32[]{:S(2)}, u32[]{:S(2)}) async-start(bf16[8,128,128]{1,2,0:T(8,128)(2,1)} %copy.34), calls=%async_computation.3 | async-start | bytes 524288 | tf_op jit(solution)/shard_map/all_to_all | solution.py:232
  82.2 8.7 %all-to-all-done.3 = bf16[8,128,128]{1,2,0:T(8,128)(2,1)S(1)} async-done(((bf16[8,128,128]{1,2,0:T(8,128)(2,1)}), bf16[8,128,128]{1,2,0:T(8,128)(2,1)S(1)}, u32[]{:S(2)}, u32[]{:S(2)}) %all-to-all-start.3) | async-done | bytes 262176 | tf_op jit(solution)/shard_map/all_to_all | solution.py:232
  90.9 2.1 fusion.37
  93.0 2.1 fusion.35
  95.1 2.1 fusion.36
  97.2 2.2 broadcast_select_fusion.7
  99.4 0.2 fusion.15
  99.6 0.4 copy-done.2
  100.0 0.8 convolution_convert_fusion
  100.8 52.1 %all_to_all.30 = bf16[32,16,2048]{2,1,0:T(8,128)(2,1)S(1)} all-to-all(bf16[32,16,2048]{2,1,0:T(8,128)(2,1)S(1)} %bitcast.95), channel_id=1, replica_groups=mesh['sp'=8,'dp'=4] {'sp','dp'}, dimensions={0} | all-to-all | bytes 4194304 | tf_op jit(solution)/shard_map/all_to_all | solution.py:269
  153.0 3.7 %fusion.4 = f32[512,1024]{1,0:T(8,128)} fusion(bf16[512,2048]{1,0:T(8,128)(2,1)S(1)} %bitcast.98, bf16[1,2048,1024]{2,1,0:T(8,128)(2,1)S(1)} %copy-done.6), kind=kOutput, calls=%fused_computation.4 | convolution fusion | flops 2147483648 | bytes 8388608 | tf_op jit(solution)/shard_map/dot_general | solution.py:277
  156.7 9.9 %fusion.6 = bf16[512,2048]{1,0:T(8,128)(2,1)} fusion(bf16[1,1024,2048]{2,1,0:T(8,128)(2,1)} %param.29, f32[512,1024]{1,0:T(8,128)} %fusion.4, bf16[512,2048]{1,0:T(8,128)(2,1)S(1)} %bitcast.99, bf16[1,2048,1024]{2,1,0:T(8,128)(2,1)} %param.28), kind=kOutput, calls=%fused_computation.6 | convolution fusion | flops 4299161600 | bytes 14680064 | tf_op jit(solution)/shard_map/dot_general | solution.py:280
  166.6 3.7 %all-to-all-start.5 = ((bf16[32,16,2048]{2,1,0:T(8,128)(2,1)}), bf16[32,16,2048]{2,1,0:T(8,128)(2,1)S(1)}, u32[]{:S(2)}, u32[]{:S(2)}) async-start(bf16[32,16,2048]{2,1,0:T(8,128)(2,1)} %bitcast.97), calls=%async_computation.5 | async-start | bytes 4194304 | tf_op jit(solution)/shard_map/all_to_all | solution.py:283
  170.7 48.3 %all-to-all-done.5 = bf16[32,16,2048]{2,1,0:T(8,128)(2,1)S(1)} async-done(((bf16[32,16,2048]{2,1,0:T(8,128)(2,1)}), bf16[32,16,2048]{2,1,0:T(8,128)(2,1)S(1)}, u32[]{:S(2)}, u32[]{:S(2)}) %all-to-all-start.5) | async-done | bytes 2097184 | tf_op jit(solution)/shard_map/all_to_all | solution.py:283
  219.0 0.5 convolution_multiply_fusion.1
  219.5 1.4 fusion.12
  (47 shorter events, 1.5 us)
Async XLA Ops:
  0.0 34.0 %copy-start.1 = (f32[1,4,1024]{2,1,0:T(4,128)S(1)}, f32[1,4,1024]{2,1,0:T(4,128)}, u32[]{:S(2)}) copy-start(f32[1,4,1024]{2,1,0:T(4,128)} %param.19) | copy-start | bytes 49156
  2.8 27.5 %all-to-all-start = ((bf16[8,384,128]{2,1,0:T(8,128)(2,1)}), bf16[8,384,128]{2,1,0:T(8,128)(2,1)S(1)}, u32[]{:S(2)}, u32[]{:S(2)}) async-start(bf16[8,384,128]{2,1,0:T(8,128)(2,1)} %get-tuple-element.7), calls=%async_computation | async-start | bytes 1572864 | tf_op jit(solution)/shard_map/all_to_all | solution.py:214
  10.0 47.4 %collective-permute-start = (bf16[2048,512]{1,0:T(8,128)(2,1)}, bf16[2048,512]{1,0:T(8,128)(2,1)}, u32[]{:S(2)}, u32[]{:S(2)}) collective-permute-start(bf16[2048,512]{1,0:T(8,128)(2,1)} %param.22), channel_id=1, source_target_pairs={{0,2},{1,3},{2,0},{3,1},{4,6},{5,7},{6,4},{7,5},{8,10},{9,11},{10,... | collective-permute-start | bytes 6291464 | tf_op jit(solution)/shard_map/ppermute | solution.py:164
  30.2 4.2 %copy-start.7 = (f32[64]{0:T(128)S(1)}, f32[64]{0:T(128)}, u32[]{:S(2)}) copy-start(f32[64]{0:T(128)} %param.20) | copy-start | bytes 772
  30.2 4.3 %copy-start.8 = (f32[64]{0:T(128)S(1)}, f32[64]{0:T(128)}, u32[]{:S(2)}) copy-start(f32[64]{0:T(128)} %param.21) | copy-start | bytes 772
  30.2 32.6 %all-to-all-start.2 = ((bf16[8,384,128]{2,1,0:T(8,128)(2,1)}), bf16[8,384,128]{2,1,0:T(8,128)(2,1)S(1)}, u32[]{:S(2)}, u32[]{:S(2)}) async-start(bf16[8,384,128]{2,1,0:T(8,128)(2,1)} %get-tuple-element.8), calls=%async_computation.2 | async-start | bytes 1572864 | tf_op jit(solution)/shard_map/all_to_all | solution.py:214
  33.9 61.1 %collective-permute-start.2 = (bf16[2048,512]{1,0:T(8,128)(2,1)}, bf16[2048,512]{1,0:T(8,128)(2,1)}, u32[]{:S(2)}, u32[]{:S(2)}) collective-permute-start(bf16[2048,512]{1,0:T(8,128)(2,1)} %param.22), channel_id=1, source_target_pairs={{0,1},{1,0},{2,3},{3,2},{4,5},{5,4},{6,7},{7,6},{8,9},{9,8},{10,11... | collective-permute-start | bytes 6291464 | tf_op jit(solution)/shard_map/ppermute | solution.py:164
  57.5 39.7 %collective-permute-start.1 = (bf16[2048,512]{1,0:T(8,128)(2,1)}, bf16[2048,512]{1,0:T(8,128)(2,1)}, u32[]{:S(2)}, u32[]{:S(2)}) collective-permute-start(bf16[2048,512]{1,0:T(8,128)(2,1)} %collective-permute-done), channel_id=1, source_target_pairs={{0,1},{1,0},{2,3},{3,2},{4,5},{5,4},{6,7},{7,6},{8,9},{9,8},{10,11... | collective-permute-start | bytes 6291464 | tf_op jit(solution)/shard_map/ppermute | solution.py:164
  57.5 11.1 %copy-start.4 = (s32[1,128,2]{1,2,0:T(2,128)S(1)}, s32[1,128,2]{1,2,0:T(2,128)}, u32[]{:S(2)}) copy-start(s32[1,128,2]{1,2,0:T(2,128)} %param.24) | copy-start | bytes 3076
  62.9 15.3 %all-to-all-start.1 = ((bf16[8,128,128]{1,2,0:T(8,128)(2,1)}), bf16[8,128,128]{1,2,0:T(8,128)(2,1)S(1)}, u32[]{:S(2)}, u32[]{:S(2)}) async-start(bf16[8,128,128]{1,2,0:T(8,128)(2,1)} %copy.33), calls=%async_computation.1 | async-start | bytes 524288 | tf_op jit(solution)/shard_map/all_to_all | solution.py:232
  78.2 12.7 %all-to-all-start.3 = ((bf16[8,128,128]{1,2,0:T(8,128)(2,1)}), bf16[8,128,128]{1,2,0:T(8,128)(2,1)S(1)}, u32[]{:S(2)}, u32[]{:S(2)}) async-start(bf16[8,128,128]{1,2,0:T(8,128)(2,1)} %copy.34), calls=%async_computation.3 | async-start | bytes 524288 | tf_op jit(solution)/shard_map/all_to_all | solution.py:232
  97.1 2.2 %copy-start = (bf16[1,128,2048]{2,1,0:T(8,128)(2,1)S(1)}, bf16[1,128,2048]{2,1,0:T(8,128)(2,1)}, u32[]{:S(2)}) copy-start(bf16[1,128,2048]{2,1,0:T(8,128)(2,1)} %param.15) | copy-start | bytes 1572868
  99.3 0.7 copy-start.2
  100.8 52.1 %copy-start.6 = (bf16[1,2048,1024]{2,1,0:T(8,128)(2,1)S(1)}, bf16[1,2048,1024]{2,1,0:T(8,128)(2,1)}, u32[]{:S(2)}) copy-start(bf16[1,2048,1024]{2,1,0:T(8,128)(2,1)} %param.27) | copy-start | bytes 12582916
  166.6 3.8 %copy-start.3 = (f32[1,128,2]{1,2,0:T(2,128)S(1)}, f32[1,128,2]{1,2,0:T(2,128)}, u32[]{:S(2)}) copy-start(f32[1,128,2]{1,2,0:T(2,128)} %param.26) | copy-start | bytes 3076
  166.6 4.0 %copy-start.5 = (f32[1,128]{1,0:T(1,128)S(1)}, f32[1,128]{1,0:T(1,128)}, u32[]{:S(2)}) copy-start(f32[1,128]{1,0:T(1,128)} %param.25) | copy-start | bytes 1540
  166.6 52.4 %all-to-all-start.5 = ((bf16[32,16,2048]{2,1,0:T(8,128)(2,1)}), bf16[32,16,2048]{2,1,0:T(8,128)(2,1)S(1)}, u32[]{:S(2)}, u32[]{:S(2)}) async-start(bf16[32,16,2048]{2,1,0:T(8,128)(2,1)} %bitcast.97), calls=%async_computation.5 | async-start | bytes 4194304 | tf_op jit(solution)/shard_map/all_to_all | solution.py:283
where the time goes:
time: 222 us; the launch traced here: 221 us
  waiting for transfers between devices  101 us (45%)
  blocking collectives  52.1 us (23%)
  starting transfers between devices  25.5 us (11%)
  matrix products  24.6 us (11%)
  Pallas kernels  11.8 us (5%)
  local copies, waits for them, and re-layouts  3.89 us (2%)
    all_to_all x1, blocking collectives, shards(): lax.all_to_all(send.reshape(experts, capacity, width), ('sp', 'dp'), spli...  52.1 us
    all_to_all x1, waiting for transfers between devices, shards(): lax.all_to_all(result.reshape(arrived.shape), ('sp', 'dp'), split_axis=0,...  48.3 us
    ppermute x3, waiting for transfers between devices, gather_shards(): held = held + [lax.ppermute(part, axis, pairs) for part in held]  22.8 us
    all_to_all x2, waiting for transfers between devices, shards(): lax.all_to_all(send, 'sp', split_axis=0, concat_axis=0, tiled=True)  18.7 us
    all_to_all x2, waiting for transfers between devices, shards(): lax.all_to_all(block.reshape(sp_size, tokens, lanes), 'sp', split_axis=0,...  11.7 us
    all_to_all x2, starting transfers between devices, shards(): lax.all_to_all(send, 'sp', split_axis=0, concat_axis=0, tiled=True)  11 us
    dot_general x1, matrix products, shards(): jnp.dot(hidden, expert_down[0], preferred_element_type=jnp.float32)  9.91 us
    all_to_all x2, starting transfers between devices, shards(): lax.all_to_all(block.reshape(sp_size, tokens, lanes), 'sp', split_axis=0,...  9.31 us
  transfers between devices with their start and end apart: 8, of which 5 were waited for; matrix products, arithmetic and copies ran while one was open for 5% of the time, Pallas kernels for 4%

commit v1 on v0

--- a/solution.py
+++ b/solution.py
@@ -17,6 +17,7 @@
 
 
 LANES = 128
+SEQ = ("hi", "lo")
 ROWS = 256
 
 
@@ -154,14 +155,39 @@
     )(qkv, gains, level, level_columns)
 
 
-def gather_shards(shard, axis):
+def tie_kernel(*refs):
+    del refs
+
+
+def tie(part, *after):
+    anywhere = pl.BlockSpec(memory_space=pl.ANY)
+    after = [array.reshape(-1, array.shape[-1])[:8, :LANES] for array in after]
+    return pl.pallas_call(
+        tie_kernel,
+        out_shape=jax.ShapeDtypeStruct(part.shape, part.dtype),
+        in_specs=[anywhere] * (1 + len(after)),
+        out_specs=anywhere,
+        input_output_aliases={0: 0},
+        name="tie",
+    )(part, *after)
+
+
+def xor_pairs(size, stride):
+    return [(index, index ^ stride) for index in range(size)]
+
+
+def gather_start(shard, axis):
     size = lax.axis_size(axis)
-    held = [shard]
-    stride = size // 2
-    offsets = [0]
+    return [shard, lax.ppermute(shard, axis, xor_pairs(size, size // 2))]
+
+
+def gather_rest(held, axis, after):
+    size = lax.axis_size(axis)
+    held = [held[0], tie(held[1], *after)]
+    offsets = [0, size // 2]
+    stride = size // 4
     while stride:
-        pairs = [(index, index ^ stride) for index in range(size)]
-        held = held + [lax.ppermute(part, axis, pairs) for part in held]
+        held = held + [lax.ppermute(part, axis, xor_pairs(size, stride)) for part in held]
         offsets = offsets + [offset ^ stride for offset in offsets]
         stride //= 2
     ordered = [None] * size
@@ -201,7 +227,7 @@
     expert_down,
 ):
     dp_size = lax.axis_size("dp")
-    sp_size = lax.axis_size("sp")
+    sp_size = lax.axis_size("hi") * lax.axis_size("lo")
     tokens = queries.shape[1]
     head_size = query_gain.shape[0]
     local_heads = forget_cache.shape[1]
@@ -211,13 +237,14 @@
     packed = lanes // head_size
     sends = pack_heads(queries[0], keys[0], values[0], sp_size, chunks, lanes)
     arrived_qkv = [
-        lax.all_to_all(send, "sp", split_axis=0, concat_axis=0, tiled=True) for send in sends
+        lax.all_to_all(send, SEQ, split_axis=0, concat_axis=0, tiled=True) for send in sends
     ]
-    weight_shards = gather_shards(out_weight, "dp")
+    weight_shards = gather_start(out_weight, "dp")
     gains = jnp.stack([jnp.tile(query_gain, packed), jnp.tile(key_gain, packed)])
     level = forget_cache[0]
     level_columns = level.T
     returned_heads = []
+    blocks = []
     for chunk in range(chunks):
         first = chunk * packed
         block = attend(
@@ -228,15 +255,17 @@
             tokens,
             head_size,
         )
+        blocks.append(block)
         returned_heads.append(
             lax.all_to_all(
                 block.reshape(sp_size, tokens, lanes),
-                "sp",
+                SEQ,
                 split_axis=0,
                 concat_axis=0,
                 tiled=True,
             )
         )
+    weight_shards = gather_rest(weight_shards, "dp", blocks)
     token_attn = (
         jnp.stack(returned_heads, axis=1)
         .transpose(2, 0, 1, 3)
@@ -250,72 +279,95 @@
     mid = (resid[0].astype(jnp.float32) + projected).astype(jnp.bfloat16)
     normed = norm_rows(mid, norm_gain)
     width = normed.shape[1]
-    tok_count = normed.shape[0]
     top_count = routes.shape[2]
-    experts = lax.axis_size("sp") * lax.axis_size("dp")
-    capacity = 2 * tok_count * top_count // experts
-    expert_ids = routes[0].reshape(-1)
-    expert_onehot = (expert_ids[:, None] == jnp.arange(experts, dtype=jnp.int32)[None, :]).astype(
-        jnp.int32
-    )
-    earlier = jnp.cumsum(expert_onehot, axis=0) - expert_onehot
-    slot_rank = jnp.sum(earlier * expert_onehot, axis=1)
-    slot_index = (expert_ids * capacity + slot_rank).reshape(tok_count, top_count)
-    slot_range = jnp.arange(experts * capacity, dtype=jnp.int32)
-    dispatch = jnp.any(slot_range[:, None, None] == slot_index[None, :, :], axis=2).astype(
-        jnp.bfloat16
-    )
-    send = jnp.dot(dispatch, normed, preferred_element_type=jnp.float32).astype(jnp.bfloat16)
-    arrived = lax.all_to_all(
-        send.reshape(experts, capacity, width),
-        ("sp", "dp"),
-        split_axis=0,
-        concat_axis=0,
-        tiled=True,
-    )
-    flat_rows = arrived.reshape(-1, width)
-    gate = jnp.dot(flat_rows, expert_gate[0], preferred_element_type=jnp.float32)
-    upper = jnp.dot(flat_rows, expert_up[0], preferred_element_type=jnp.float32)
-    hidden = (jax.nn.silu(gate) * upper).astype(jnp.bfloat16)
-    result = jnp.dot(hidden, expert_down[0], preferred_element_type=jnp.float32).astype(
-        jnp.bfloat16
-    )
-    returned = lax.all_to_all(
-        result.reshape(arrived.shape), ("sp", "dp"), split_axis=0, concat_axis=0, tiled=True
-    )
-    returned = returned.reshape(experts * capacity, width)
+    swap = [(0, 1), (1, 0)]
+    half = sp_size * dp_size // 2
+    capacity = tokens * top_count // half
     shares = inner_share[0]
     weights = group_weight[0][:, None] * shares / jnp.sum(shares, axis=-1, keepdims=True)
-    mixed = jnp.zeros((tok_count, width), jnp.float32)
-    for route in range(top_count):
-        select = (slot_range[None, :] == slot_index[:, route : route + 1]).astype(jnp.bfloat16)
-        picked = jnp.dot(select, returned, preferred_element_type=jnp.float32)
+    own_slots = slots_of(routes[0], half, capacity)
+    far_slots = slots_of(lax.ppermute(routes[0], "hi", swap), half, capacity)
+    far_weights = lax.ppermute(weights, "hi", swap)
+    far_normed = lax.ppermute(normed, "hi", swap)
+    experts = (expert_gate[0], expert_up[0], expert_down[0])
+    own_rows = exchange(spread(normed, own_slots, half, capacity))
+    far_normed = tie(far_normed, own_rows)
+    far_rows = exchange(spread(far_normed, far_slots, half, capacity))
+    own_result = expert_of(own_rows, *experts)
+    far_back = exchange(expert_of(far_rows, *experts))
+    own_back = exchange(tie(own_result, far_back))
+    far_mixed = gather_back(far_back, far_slots, far_weights).astype(jnp.bfloat16)
+    other = lax.ppermute(far_mixed, "hi", swap)
+    mixed = gather_back(own_back, own_slots, weights) + other.astype(jnp.float32)
+    layer_out = (mid.astype(jnp.float32) + mixed).astype(jnp.bfloat16)
+    return layer_out.reshape(1, tokens, width)
+
+
+def slots_of(ids, half, capacity):
+    tok_count, top_count = ids.shape
+    flat = ids.reshape(-1)
+    onehot = (flat[:, None] == jnp.arange(2 * half, dtype=jnp.int32)[None, :]).astype(jnp.int32)
+    earlier = jnp.cumsum(onehot, axis=0) - onehot
+    rank = jnp.sum(earlier * onehot, axis=1)
+    return ((flat - lax.axis_index("hi") * half) * capacity + rank).reshape(tok_count, top_count)
+
+
+def spread(rows, slots, half, capacity):
+    slot_range = jnp.arange(half * capacity, dtype=jnp.int32)
+    dispatch = jnp.any(slot_range[:, None, None] == slots[None, :, :], axis=2)
+    send = jnp.dot(dispatch.astype(jnp.bfloat16), rows, preferred_element_type=jnp.float32)
+    return send.astype(jnp.bfloat16).reshape(half, capacity, rows.shape[1])
+
+
+def exchange(rows):
+    return lax.all_to_all(rows, ("lo", "dp"), split_axis=0, concat_axis=0, tiled=True)
+
+
+def expert_of(rows, gate_weight, up_weight, down_weight):
+    flat = rows.reshape(-1, rows.shape[2])
+    gate = jnp.dot(flat, gate_weight, preferred_element_type=jnp.float32)
+    upper = jnp.dot(flat, up_weight, preferred_element_type=jnp.float32)
+    hidden = (jax.nn.silu(gate) * upper).astype(jnp.bfloat16)
+    result = jnp.dot(hidden, down_weight, preferred_element_type=jnp.float32)
+    return result.astype(jnp.bfloat16).reshape(rows.shape)
+
+
+def gather_back(returned, slots, weights):
+    flat = returned.reshape(-1, returned.shape[2])
+    slot_range = jnp.arange(flat.shape[0], dtype=jnp.int32)
+    mixed = jnp.zeros((slots.shape[0], flat.shape[1]), jnp.float32)
+    for route in range(slots.shape[1]):
+        select = (slot_range[None, :] == slots[:, route : route + 1]).astype(jnp.bfloat16)
+        picked = jnp.dot(select, flat, preferred_element_type=jnp.float32)
         mixed = mixed + weights[:, route : route + 1] * picked
-    layer_out = (mid.astype(jnp.float32) + mixed).astype(jnp.bfloat16)
-    return layer_out.reshape(1, tok_count, width)
+    return mixed
 
 
 def solution(mesh):
+    sizes = mesh.shape
+    mesh = jax.sharding.Mesh(
+        mesh.devices.reshape(2, sizes["sp"] // 2, sizes["dp"]), ("hi", "lo", "dp")
+    )
     return jax.shard_map(
         shards,
         mesh=mesh,
         in_specs=(
-            P("dp", "sp", None),
-            P("dp", "sp", None),
-            P("dp", "sp", None),
-            P("dp", "sp", None),
-            P("dp", "sp", None),
+            P("dp", SEQ, None),
+            P("dp", SEQ, None),
+            P("dp", SEQ, None),
+            P("dp", SEQ, None),
+            P("dp", SEQ, None),
             P(),
             P(),
             P(None, "dp"),
             P(),
-            P("dp", "sp", None),
-            P("dp", "sp"),
-            P("dp", "sp", None),
-            P(("sp", "dp"), None, None),
-            P(("sp", "dp"), None, None),
-            P(("sp", "dp"), None, None),
+            P("dp", SEQ, None),
+            P("dp", SEQ),
+            P("dp", SEQ, None),
+            P(("hi", "lo", "dp"), None, None),
+            P(("hi", "lo", "dp"), None, None),
+            P(("hi", "lo", "dp"), None, None),
         ),
-        out_specs=P("dp", "sp", None),
+        out_specs=P("dp", SEQ, None),
         check_vma=False,
     )

time: 222 us -> 239 us (1.077)
  blocking collectives: 52.1 us -> 19.4 us
  waiting for transfers between devices: 101 us -> 120 us
  starting transfers between devices: 25.5 us -> 41.8 us
  matrix products: 24.6 us -> 34.4 us
  local copies, waits for them, and re-layouts: 3.89 us -> 7.39 us
    ppermute x3 -> x7, waiting for transfers between devices: 22.8 us -> 65.6 us  [the longest x1 22.1 us: shards(): other = lax.ppermute(far_mixed, 'hi', swap)]
    all_to_all x1, blocking collectives: 52.1 us -> 19.4 us  [exchange(): lax.all_to_all(rows, ('lo', 'dp'), split_axis=0, concat_axis=0, tiled=True)]
    all_to_all x5 -> x7, waiting for transfers between devices: 78.6 us -> 53.9 us  [the longest x2 33.2 us: shards(): lax.all_to_all(send, SEQ, split_axis=0, concat_axis=0, tiled=True)]
    dot_general x5 -> x10, matrix products: 16.2 us -> 27.6 us  [the longest x2 14.5 us: expert_of(): result = jnp.dot(hidden, down_weight, preferred_element_type=jnp.float32)]
    ppermute x3 -> x7, starting transfers between devices: 1.59 us -> 12.4 us  [the longest x1 3.43 us: shards(): far_normed = lax.ppermute(normed, 'hi', swap)]
    all_to_all x5 -> x7, starting transfers between devices: 24 us -> 29.4 us  [the longest x3 11.1 us: exchange(): lax.all_to_all(rows, ('lo', 'dp'), split_axis=0, concat_axis=0, tiled=True)]
    slice x2 -> x7, local copies, waits for them, and re-layouts: 0.36 us -> 2.87 us  [the longest x4 2.34 us: tie(): after = [array.reshape(-1, array.shape[-1])[:8, :LANES] for array in after]]
  transfers between devices with their start and end apart: 8 -> 14, of which waited for: 5 -> 9; matrix products, arithmetic and copies ran while one was open for 5% -> 11% of each run, Pallas kernels for 4% -> 4%
where the time goes in v1:
time: 239 us; the launch traced here: 238 us
  waiting for transfers between devices  120 us (50%)
  starting transfers between devices  41.8 us (17%)
  matrix products  34.4 us (14%)
  blocking collectives  19.4 us (8%)
  Pallas kernels  11.8 us (5%)
  local copies, waits for them, and re-layouts  7.39 us (3%)
  other arithmetic  3.11 us (1%)
    all_to_all x2, waiting for transfers between devices, shards(): lax.all_to_all(send, SEQ, split_axis=0, concat_axis=0, tiled=True)  33.2 us
    ppermute x1, waiting for transfers between devices, shards(): other = lax.ppermute(far_mixed, 'hi', swap)  22.1 us
    ppermute x1, waiting for transfers between devices, shards(): far_normed = lax.ppermute(normed, 'hi', swap)  21.9 us
    all_to_all x1, blocking collectives, exchange(): lax.all_to_all(rows, ('lo', 'dp'), split_axis=0, concat_axis=0, tiled=True)  19.4 us
    all_to_all x2, waiting for transfers between devices, shards(): lax.all_to_all(block.reshape(sp_size, tokens, lanes), SEQ, split_axis=0,...  16.3 us
    dot_general x2, matrix products, expert_of(): result = jnp.dot(hidden, down_weight, preferred_element_type=jnp.float32)  14.5 us
    ppermute x1, waiting for transfers between devices, shards(): far_slots = slots_of(lax.ppermute(routes[0], 'hi', swap), half, capacity)  12.2 us
    all_to_all x3, starting transfers between devices, exchange(): lax.all_to_all(rows, ('lo', 'dp'), split_axis=0, concat_axis=0, tiled=True)  11.1 us
  transfers between devices with their start and end apart: 14, of which 9 were waited for; matrix products, arithmetic and copies ran while one was open for 11% of the time, Pallas kernels for 4%

profile of v1, /device:TPU:0, one launch (start us, length us, event | category | flops | bytes accessed | tf_op | source)
XLA Modules:
  0.0 237.7 jit_solution(15391082116040378563)
XLA Ops:
  0.0 2.8 %pack_heads.1 = (bf16[8,384,128]{2,1,0:T(8,128)(2,1)}, bf16[8,384,128]{2,1,0:T(8,128)(2,1)}) custom-call(bf16[128,2048]{1,0:T(8,128)(2,1)} %bitcast.160, bf16[128,2048]{1,0:T(8,128)(2,1)} %bitcast.161, bf16[128,2048]{1,0:T(8,128)(2,1)} %bitcast.162), custom_call_target="tpu_custom_call" | custom-call | flops 262144 | bytes 3145728 | tf_op jit(solution)/shard_map/pack_heads/pallas_call | solution.py:40
  2.8 7.3 %all-to-all-start = ((bf16[8,384,128]{2,1,0:T(8,128)(2,1)}), bf16[8,384,128]{2,1,0:T(8,128)(2,1)S(1)}, u32[]{:S(2)}, u32[]{:S(2)}) async-start(bf16[8,384,128]{2,1,0:T(8,128)(2,1)} %get-tuple-element.7), calls=%async_computation | async-start | bytes 1572864 | tf_op jit(solution)/shard_map/all_to_all | solution.py:240
  10.1 1.5 collective-permute-start
  11.6 18.7 %all-to-all-done.qkv_ref = bf16[8,384,128]{2,1,0:T(8,128)(2,1)S(1)} async-done(((bf16[8,384,128]{2,1,0:T(8,128)(2,1)}), bf16[8,384,128]{2,1,0:T(8,128)(2,1)S(1)}, u32[]{:S(2)}, u32[]{:S(2)}) %all-to-all-start) | async-done | bytes 786464 | tf_op jit(solution)/shard_map/all_to_all | solution.py:240
  30.2 3.6 %all-to-all-start.2 = ((bf16[8,384,128]{2,1,0:T(8,128)(2,1)}), bf16[8,384,128]{2,1,0:T(8,128)(2,1)S(1)}, u32[]{:S(2)}, u32[]{:S(2)}) async-start(bf16[8,384,128]{2,1,0:T(8,128)(2,1)} %get-tuple-element.8), calls=%async_computation.2 | async-start | bytes 1572864 | tf_op jit(solution)/shard_map/all_to_all | solution.py:240
  34.5 4.5 %attend.2 = bf16[1024,128]{1,0:T(8,128)(2,1)S(1)} custom-call(bf16[8,384,128]{2,1,0:T(8,128)(2,1)S(1)} %all-to-all-done.qkv_ref, f32[2,128]{1,0:T(2,128)S(1)} %pad_maximum_fusion.1.gains_ref, f32[2,1024]{1,0:T(2,128)S(1)} %get-tuple-element.21.level_ref, f32[1024,2]{1,0:T(8,128)S(1)} %get-tuple-element.19.column_ref), custom_call_target="tpu_custom_call" | custom-call | flops 1073741824 | bytes 1048576 | tf_op jit(solution)/shard_map/attend/pallas_call | solution.py:140
  39.6 14.6 %all-to-all-done.2.qkv_ref = bf16[8,384,128]{2,1,0:T(8,128)(2,1)S(1)} async-done(((bf16[8,384,128]{2,1,0:T(8,128)(2,1)}), bf16[8,384,128]{2,1,0:T(8,128)(2,1)S(1)}, u32[]{:S(2)}, u32[]{:S(2)}) %all-to-all-start.2) | async-done | bytes 786464 | tf_op jit(solution)/shard_map/all_to_all | solution.py:240
  54.2 4.5 %attend.3 = bf16[1024,128]{1,0:T(8,128)(2,1)S(1)} custom-call(bf16[8,384,128]{2,1,0:T(8,128)(2,1)S(1)} %all-to-all-done.2.qkv_ref, f32[2,128]{1,0:T(2,128)S(1)} %pad_maximum_fusion.1.gains_ref, f32[2,1024]{1,0:T(2,128)S(1)} %get-tuple-element.22.level_ref, f32[1024,2]{1,0:T(8,128)S(1)} %get-tuple-element.20.column_ref), custom_call_target="tpu_custom_call" | custom-call | flops 1073741824 | bytes 1048576 | tf_op jit(solution)/shard_map/attend/pallas_call | solution.py:140
  60.1 3.9 %all-to-all-start.3 = ((bf16[8,128,128]{1,2,0:T(8,128)(2,1)}), bf16[8,128,128]{1,2,0:T(8,128)(2,1)S(1)}, u32[]{:S(2)}, u32[]{:S(2)}) async-start(bf16[8,128,128]{1,2,0:T(8,128)(2,1)} %copy.59), calls=%async_computation.3 | async-start | bytes 524288 | tf_op jit(solution)/shard_map/all_to_all | solution.py:260
  65.8 7.9 %all-to-all-done.3 = bf16[8,128,128]{1,2,0:T(8,128)(2,1)S(1)} async-done(((bf16[8,128,128]{1,2,0:T(8,128)(2,1)}), bf16[8,128,128]{1,2,0:T(8,128)(2,1)S(1)}, u32[]{:S(2)}, u32[]{:S(2)}) %all-to-all-start.3) | async-done | bytes 262176 | tf_op jit(solution)/shard_map/all_to_all | solution.py:260
  73.6 3.6 %all-to-all-start.1 = ((bf16[8,128,128]{1,2,0:T(8,128)(2,1)}), bf16[8,128,128]{1,2,0:T(8,128)(2,1)S(1)}, u32[]{:S(2)}, u32[]{:S(2)}) async-start(bf16[8,128,128]{1,2,0:T(8,128)(2,1)} %copy.58), calls=%async_computation.1 | async-start | bytes 524288 | tf_op jit(solution)/shard_map/all_to_all | solution.py:260
  78.0 8.4 %all-to-all-done.1 = bf16[8,128,128]{1,2,0:T(8,128)(2,1)S(1)} async-done(((bf16[8,128,128]{1,2,0:T(8,128)(2,1)}), bf16[8,128,128]{1,2,0:T(8,128)(2,1)S(1)}, u32[]{:S(2)}, u32[]{:S(2)}) %all-to-all-start.1) | async-done | bytes 262176 | tf_op jit(solution)/shard_map/all_to_all | solution.py:260
  86.4 2.1 fusion.66
  88.5 2.1 fusion.64
  90.6 2.1 fusion.65
  95.1 3.7 %all-to-all-start.4 = ((bf16[16,16,2048]{2,1,0:T(8,128)(2,1)}), bf16[16,16,2048]{2,1,0:T(8,128)(2,1)S(1)}, u32[]{:S(2)}, u32[]{:S(2)}) async-start(bf16[16,16,2048]{2,1,0:T(8,128)(2,1)} %bitcast.22), calls=%async_computation.4 | async-start | bytes 2097152 | tf_op jit(solution)/shard_map/all_to_all | solution.py:323
  98.9 1.5 collective-permute-start.3
  100.4 12.2 %collective-permute-done.3 = s32[128,2]{1,0:T(8,128)S(1)} collective-permute-done((s32[128,2]{1,0:T(8,128)S(1)}, s32[128,2]{1,0:T(8,128)S(1)}, u32[]{:S(2)}, u32[]{:S(2)}) %collective-permute-start.3) | collective-permute-done | bytes 1056 | tf_op jit(solution)/shard_map/ppermute | solution.py:289
  113.4 3.4 %collective-permute-start.4 = (bf16[128,2048]{1,0:T(8,128)(2,1)S(1)}, bf16[128,2048]{1,0:T(8,128)(2,1)S(1)}, u32[]{:S(2)}, u32[]{:S(2)}) collective-permute-start(bf16[128,2048]{1,0:T(8,128)(2,1)S(1)} %fusion.33), channel_id=1, source_target_pairs={{0,16},{16,0},{1,17},{17,1},{2,18},{18,2},{3,19},{19,3},{4,20},{20... | collective-permute-start | bytes 1572872 | tf_op jit(solution)/shard_map/ppermute | solution.py:291
  118.2 21.9 %collective-permute-done.4.refs_0_ = bf16[128,2048]{1,0:T(8,128)(2,1)S(1)} collective-permute-done((bf16[128,2048]{1,0:T(8,128)(2,1)S(1)}, bf16[128,2048]{1,0:T(8,128)(2,1)S(1)}, u32[]{:S(2)}, u32[]{:S(2)}) %collective-permute-start.4) | collective-permute-done | bytes 524320 | tf_op jit(solution)/shard_map/ppermute | solution.py:291
  142.3 19.4 %all_to_all.40 = bf16[16,16,2048]{2,1,0:T(8,128)(2,1)S(1)} all-to-all(bf16[16,16,2048]{2,1,0:T(8,128)(2,1)S(1)} %bitcast.150), channel_id=1, replica_groups=mesh['hi'=2,'lo'=4,'dp'=4] {'lo','dp'}, dimensions={0} | all-to-all | bytes 2097152 | tf_op jit(solution)/shard_map/all_to_all | solution.py:323
  161.7 4.5 %fusion.8 = f32[256,1024]{1,0:T(8,128)} fusion(bf16[256,2048]{1,0:T(8,128)(2,1)S(1)} %bitcast.156, bf16[1,2048,1024]{2,1,0:T(8,128)(2,1)} %param.27), kind=kOutput, calls=%fused_computation.8 | convolution fusion | flops 1073741824 | bytes 6291456 | tf_op jit(solution)/shard_map/dot_general | solution.py:328
  166.2 7.2 %fusion.15 = bf16[256,2048]{1,0:T(8,128)(2,1)} fusion(bf16[1,1024,2048]{2,1,0:T(8,128)(2,1)} %param.29, bf16[256,2048]{1,0:T(8,128)(2,1)S(1)} %bitcast.157, bf16[1,2048,1024]{2,1,0:T(8,128)(2,1)} %param.28, f32[256,1024]{1,0:T(8,128)} %fusion.8), kind=kOutput, calls=%fused_computation.15 | convolution fusion | flops 2149580800 | bytes 11534336 | tf_op jit(solution)/shard_map/dot_general | solution.py:331
  173.4 3.7 %all-to-all-start.6 = ((bf16[16,16,2048]{2,1,0:T(8,128)(2,1)}), bf16[16,16,2048]{2,1,0:T(8,128)(2,1)S(1)}, u32[]{:S(2)}, u32[]{:S(2)}) async-start(bf16[16,16,2048]{2,1,0:T(8,128)(2,1)} %bitcast.155), calls=%async_computation.6 | async-start | bytes 2097152 | tf_op jit(solution)/shard_map/all_to_all | solution.py:323
  177.0 4.4 %fusion.10 = f32[256,1024]{1,0:T(8,128)} fusion(bf16[256,2048]{1,0:T(8,128)(2,1)S(1)} %bitcast.152, bf16[1,2048,1024]{2,1,0:T(8,128)(2,1)} %param.27), kind=kOutput, calls=%fused_computation.10 | convolution fusion | flops 1073741824 | bytes 6291456 | tf_op jit(solution)/shard_map/dot_general | solution.py:328
  181.5 7.3 %fusion.12 = bf16[256,2048]{1,0:T(8,128)(2,1)} fusion(bf16[1,1024,2048]{2,1,0:T(8,128)(2,1)} %param.29, bf16[256,2048]{1,0:T(8,128)(2,1)S(1)} %bitcast.153, bf16[1,2048,1024]{2,1,0:T(8,128)(2,1)} %param.28, f32[256,1024]{1,0:T(8,128)} %fusion.10), kind=kOutput, calls=%fused_computation.14 | convolution fusion | flops 2149580800 | bytes 11534336 | tf_op jit(solution)/shard_map/dot_general | solution.py:331
  188.7 4.5 %all-to-all-done.6 = bf16[16,16,2048]{2,1,0:T(8,128)(2,1)S(1)} async-done(((bf16[16,16,2048]{2,1,0:T(8,128)(2,1)}), bf16[16,16,2048]{2,1,0:T(8,128)(2,1)S(1)}, u32[]{:S(2)}, u32[]{:S(2)}) %all-to-all-start.6) | async-done | bytes 1048608 | tf_op jit(solution)/shard_map/all_to_all | solution.py:323
  193.8 3.7 %all-to-all-start.7 = ((bf16[16,16,2048]{2,1,0:T(8,128)(2,1)}), bf16[16,16,2048]{2,1,0:T(8,128)(2,1)S(1)}, u32[]{:S(2)}, u32[]{:S(2)}) async-start(bf16[16,16,2048]{2,1,0:T(8,128)(2,1)} %tie.5), calls=%async_computation.7 | async-start | bytes 2097152 | tf_op jit(solution)/shard_map/all_to_all | solution.py:323
  197.5 2.4 %collective-permute-start.5 = (f32[128,2]{0,1:T(2,128)S(1)}, f32[128,2]{0,1:T(2,128)S(1)}, u32[]{:S(2)}, u32[]{:S(2)}) collective-permute-start(f32[128,2]{0,1:T(2,128)S(1)} %fusion.59), channel_id=1, source_target_pairs={{0,16},{16,0},{1,17},{17,1},{2,18},{18,2},{3,19},{19,3},{4,20},{20... | collective-permute-start | bytes 3080 | tf_op jit(solution)/shard_map/ppermute | solution.py:290
  200.5 9.3 %collective-permute-done.5 = f32[128,2]{0,1:T(2,128)S(1)} collective-permute-done((f32[128,2]{0,1:T(2,128)S(1)}, f32[128,2]{0,1:T(2,128)S(1)}, u32[]{:S(2)}, u32[]{:S(2)}) %collective-permute-start.5) | collective-permute-done | bytes 1056 | tf_op jit(solution)/shard_map/ppermute | solution.py:290
  210.5 3.3 %collective-permute-start.6 = (bf16[128,2048]{1,0:T(8,128)(2,1)S(1)}, bf16[128,2048]{1,0:T(8,128)(2,1)S(1)}, u32[]{:S(2)}, u32[]{:S(2)}) collective-permute-start(bf16[128,2048]{1,0:T(8,128)(2,1)S(1)} %add_convert_fusion), channel_id=1, source_target_pairs={{0,16},{16,0},{1,17},{17,1},{2,18},{18,2},{3,19},{19,3},{4,20},{20... | collective-permute-start | bytes 1572872 | tf_op jit(solution)/shard_map/ppermute | solution.py:300
  214.5 22.1 %collective-permute-done.6 = bf16[128,2048]{1,0:T(8,128)(2,1)S(1)} collective-permute-done((bf16[128,2048]{1,0:T(8,128)(2,1)S(1)}, bf16[128,2048]{1,0:T(8,128)(2,1)S(1)}, u32[]{:S(2)}, u32[]{:S(2)}) %collective-permute-start.6) | collective-permute-done | bytes 524320 | tf_op jit(solution)/shard_map/ppermute | solution.py:300
  (87 shorter events, 15.4 us)
Async XLA Ops:
  0.0 33.9 %copy-start.2 = (f32[1,4,1024]{2,1,0:T(4,128)S(1)}, f32[1,4,1024]{2,1,0:T(4,128)}, u32[]{:S(2)}) copy-start(f32[1,4,1024]{2,1,0:T(4,128)} %param.19) | copy-start | bytes 49156
  0.0 34.1 %copy-start.7 = (f32[64]{0:T(128)S(1)}, f32[64]{0:T(128)}, u32[]{:S(2)}) copy-start(f32[64]{0:T(128)} %param.20) | copy-start | bytes 772
  0.0 34.2 %copy-start.8 = (f32[64]{0:T(128)S(1)}, f32[64]{0:T(128)}, u32[]{:S(2)}) copy-start(f32[64]{0:T(128)} %param.21) | copy-start | bytes 772
  2.8 27.5 %all-to-all-start = ((bf16[8,384,128]{2,1,0:T(8,128)(2,1)}), bf16[8,384,128]{2,1,0:T(8,128)(2,1)S(1)}, u32[]{:S(2)}, u32[]{:S(2)}) async-start(bf16[8,384,128]{2,1,0:T(8,128)(2,1)} %get-tuple-element.7), calls=%async_computation | async-start | bytes 1572864 | tf_op jit(solution)/shard_map/all_to_all | solution.py:240
  10.1 49.2 %collective-permute-start = (bf16[2048,512]{1,0:T(8,128)(2,1)}, bf16[2048,512]{1,0:T(8,128)(2,1)}, u32[]{:S(2)}, u32[]{:S(2)}) collective-permute-start(bf16[2048,512]{1,0:T(8,128)(2,1)} %param.22), channel_id=1, source_target_pairs={{0,2},{1,3},{2,0},{3,1},{4,6},{5,7},{6,4},{7,5},{8,10},{9,11},{10,... | collective-permute-start | bytes 6291464 | tf_op jit(solution)/shard_map/ppermute | solution.py:181
  30.2 24.0 %all-to-all-start.2 = ((bf16[8,384,128]{2,1,0:T(8,128)(2,1)}), bf16[8,384,128]{2,1,0:T(8,128)(2,1)S(1)}, u32[]{:S(2)}, u32[]{:S(2)}) async-start(bf16[8,384,128]{2,1,0:T(8,128)(2,1)} %get-tuple-element.8), calls=%async_computation.2 | async-start | bytes 1572864 | tf_op jit(solution)/shard_map/all_to_all | solution.py:240
  33.8 56.8 %collective-permute-start.2 = (bf16[2048,512]{1,0:T(8,128)(2,1)}, bf16[2048,512]{1,0:T(8,128)(2,1)}, u32[]{:S(2)}, u32[]{:S(2)}) collective-permute-start(bf16[2048,512]{1,0:T(8,128)(2,1)} %param.22), channel_id=1, source_target_pairs={{0,1},{1,0},{2,3},{3,2},{4,5},{5,4},{6,7},{7,6},{8,9},{9,8},{10,11... | collective-permute-start | bytes 6291464 | tf_op jit(solution)/shard_map/ppermute | solution.py:190
  54.2 9.9 %copy-start.4 = (s32[1,128,2]{1,2,0:T(2,128)S(1)}, s32[1,128,2]{1,2,0:T(2,128)}, u32[]{:S(2)}) copy-start(s32[1,128,2]{1,2,0:T(2,128)} %param.24) | copy-start | bytes 3076
  59.3 33.4 %collective-permute-start.1 = (bf16[2048,512]{1,0:T(8,128)(2,1)}, bf16[2048,512]{1,0:T(8,128)(2,1)S(1)}, u32[]{:S(2)}, u32[]{:S(2)}) collective-permute-start(bf16[2048,512]{1,0:T(8,128)(2,1)} %tie.3), channel_id=1, source_target_pairs={{0,1},{1,0},{2,3},{3,2},{4,5},{5,4},{6,7},{7,6},{8,9},{9,8},{10,11... | collective-permute-start | bytes 6291464 | tf_op jit(solution)/shard_map/ppermute | solution.py:190
  60.1 13.5 %all-to-all-start.3 = ((bf16[8,128,128]{1,2,0:T(8,128)(2,1)}), bf16[8,128,128]{1,2,0:T(8,128)(2,1)S(1)}, u32[]{:S(2)}, u32[]{:S(2)}) async-start(bf16[8,128,128]{1,2,0:T(8,128)(2,1)} %copy.59), calls=%async_computation.3 | async-start | bytes 524288 | tf_op jit(solution)/shard_map/all_to_all | solution.py:260
  73.6 12.7 %all-to-all-start.1 = ((bf16[8,128,128]{1,2,0:T(8,128)(2,1)}), bf16[8,128,128]{1,2,0:T(8,128)(2,1)S(1)}, u32[]{:S(2)}, u32[]{:S(2)}) async-start(bf16[8,128,128]{1,2,0:T(8,128)(2,1)} %copy.58), calls=%async_computation.1 | async-start | bytes 524288 | tf_op jit(solution)/shard_map/all_to_all | solution.py:260
  90.5 2.7 %copy-start.1 = (bf16[1,128,2048]{2,1,0:T(8,128)(2,1)S(1)}, bf16[1,128,2048]{2,1,0:T(8,128)(2,1)}, u32[]{:S(2)}) copy-start(bf16[1,128,2048]{2,1,0:T(8,128)(2,1)} %param.15) | copy-start | bytes 1572868
  90.5 2.9 %copy-start.3 = (f32[2048]{0:T(1024)S(1)}, f32[2048]{0:T(1024)}, u32[]{:S(2)}) copy-start(f32[2048]{0:T(1024)} %param.23) | copy-start | bytes 24580
  95.1 22.5 %all-to-all-start.4 = ((bf16[16,16,2048]{2,1,0:T(8,128)(2,1)}), bf16[16,16,2048]{2,1,0:T(8,128)(2,1)S(1)}, u32[]{:S(2)}, u32[]{:S(2)}) async-start(bf16[16,16,2048]{2,1,0:T(8,128)(2,1)} %bitcast.22), calls=%async_computation.4 | async-start | bytes 2097152 | tf_op jit(solution)/shard_map/all_to_all | solution.py:323
  98.9 13.8 %collective-permute-start.3 = (s32[128,2]{1,0:T(8,128)S(1)}, s32[128,2]{1,0:T(8,128)S(1)}, u32[]{:S(2)}, u32[]{:S(2)}) collective-permute-start(s32[128,2]{1,0:T(8,128)S(1)} %bitcast.154), channel_id=1, source_target_pairs={{0,16},{16,0},{1,17},{17,1},{2,18},{18,2},{3,19},{19,3},{4,20},{20... | collective-permute-start | bytes 3080 | tf_op jit(solution)/shard_map/ppermute | solution.py:289
  113.4 26.7 %collective-permute-start.4 = (bf16[128,2048]{1,0:T(8,128)(2,1)S(1)}, bf16[128,2048]{1,0:T(8,128)(2,1)S(1)}, u32[]{:S(2)}, u32[]{:S(2)}) collective-permute-start(bf16[128,2048]{1,0:T(8,128)(2,1)S(1)} %fusion.33), channel_id=1, source_target_pairs={{0,16},{16,0},{1,17},{17,1},{2,18},{18,2},{3,19},{19,3},{4,20},{20... | collective-permute-start | bytes 1572872 | tf_op jit(solution)/shard_map/ppermute | solution.py:291
  140.1 0.8 copy-start
  173.4 19.8 %all-to-all-start.6 = ((bf16[16,16,2048]{2,1,0:T(8,128)(2,1)}), bf16[16,16,2048]{2,1,0:T(8,128)(2,1)S(1)}, u32[]{:S(2)}, u32[]{:S(2)}) async-start(bf16[16,16,2048]{2,1,0:T(8,128)(2,1)} %bitcast.155), calls=%async_computation.6 | async-start | bytes 2097152 | tf_op jit(solution)/shard_map/all_to_all | solution.py:323
  188.7 8.7 %copy-start.5 = (f32[1,128,2]{1,2,0:T(2,128)S(1)}, f32[1,128,2]{1,2,0:T(2,128)}, u32[]{:S(2)}) copy-start(f32[1,128,2]{1,2,0:T(2,128)} %param.26) | copy-start | bytes 3076
  188.7 8.7 %copy-start.6 = (f32[1,128]{1,0:T(1,128)S(1)}, f32[1,128]{1,0:T(1,128)}, u32[]{:S(2)}) copy-start(f32[1,128]{1,0:T(1,128)} %param.25) | copy-start | bytes 1540
  193.8 20.1 %all-to-all-start.7 = ((bf16[16,16,2048]{2,1,0:T(8,128)(2,1)}), bf16[16,16,2048]{2,1,0:T(8,128)(2,1)S(1)}, u32[]{:S(2)}, u32[]{:S(2)}) async-start(bf16[16,16,2048]{2,1,0:T(8,128)(2,1)} %tie.5), calls=%async_computation.7 | async-start | bytes 2097152 | tf_op jit(solution)/shard_map/all_to_all | solution.py:323
  197.5 12.3 %collective-permute-start.5 = (f32[128,2]{0,1:T(2,128)S(1)}, f32[128,2]{0,1:T(2,128)S(1)}, u32[]{:S(2)}, u32[]{:S(2)}) collective-permute-start(f32[128,2]{0,1:T(2,128)S(1)} %fusion.59), channel_id=1, source_target_pairs={{0,16},{16,0},{1,17},{17,1},{2,18},{18,2},{3,19},{19,3},{4,20},{20... | collective-permute-start | bytes 3080 | tf_op jit(solution)/shard_map/ppermute | solution.py:290
  210.5 26.2 %collective-permute-start.6 = (bf16[128,2048]{1,0:T(8,128)(2,1)S(1)}, bf16[128,2048]{1,0:T(8,128)(2,1)S(1)}, u32[]{:S(2)}, u32[]{:S(2)}) collective-permute-start(bf16[128,2048]{1,0:T(8,128)(2,1)S(1)} %add_convert_fusion), channel_id=1, source_target_pairs={{0,16},{16,0},{1,17},{17,1},{2,18},{18,2},{3,19},{19,3},{4,20},{20... | collective-permute-start | bytes 1572872 | tf_op jit(solution)/shard_map/ppermute | solution.py:300

commit v2 on v0

--- a/solution.py
+++ b/solution.py
@@ -17,7 +17,9 @@
 
 
 LANES = 128
+SEQ = "sp"
 ROWS = 256
+UNITS = 256
 
 
 def pack_kernel(query_ref, key_ref, value_ref, *out_refs):
@@ -154,14 +156,39 @@
     )(qkv, gains, level, level_columns)
 
 
-def gather_shards(shard, axis):
+def tie_kernel(*refs):
+    del refs
+
+
+def tie(part, *after):
+    anywhere = pl.BlockSpec(memory_space=pl.ANY)
+    after = [array.reshape(-1, array.shape[-1])[:8, :LANES] for array in after]
+    return pl.pallas_call(
+        tie_kernel,
+        out_shape=jax.ShapeDtypeStruct(part.shape, part.dtype),
+        in_specs=[anywhere] * (1 + len(after)),
+        out_specs=anywhere,
+        input_output_aliases={0: 0},
+        name="tie",
+    )(part, *after)
+
+
+def xor_pairs(size, stride):
+    return [(index, index ^ stride) for index in range(size)]
+
+
+def gather_start(shard, axis):
     size = lax.axis_size(axis)
-    held = [shard]
-    stride = size // 2
-    offsets = [0]
+    return [shard, lax.ppermute(shard, axis, xor_pairs(size, size // 2))]
+
+
+def gather_rest(held, axis, after):
+    size = lax.axis_size(axis)
+    held = [held[0], tie(held[1], *after)]
+    offsets = [0, size // 2]
+    stride = size // 4
     while stride:
-        pairs = [(index, index ^ stride) for index in range(size)]
-        held = held + [lax.ppermute(part, axis, pairs) for part in held]
+        held = held + [lax.ppermute(part, axis, xor_pairs(size, stride)) for part in held]
         offsets = offsets + [offset ^ stride for offset in offsets]
         stride //= 2
     ordered = [None] * size
@@ -181,6 +208,53 @@
         ]
         stride *= 2
     return pieces
+
+
+def expert_kernel(rows_ref, gate_ref, up_ref, down_ref, out_ref, total_ref):
+    step = pl.program_id(0)
+    rows = rows_ref[...]
+    gate = jnp.dot(rows, gate_ref[...], preferred_element_type=jnp.float32)
+    upper = jnp.dot(rows, up_ref[...], preferred_element_type=jnp.float32)
+    hidden = (gate / (1.0 + jnp.exp(-gate)) * upper).astype(jnp.bfloat16)
+    part = jnp.dot(hidden, down_ref[...], preferred_element_type=jnp.float32)
+
+    @pl.when(step == 0)
+    def _():
+        total_ref[...] = part
+
+    @pl.when(step > 0)
+    def _():
+        total_ref[...] += part
+
+    @pl.when(step == pl.num_programs(0) - 1)
+    def _():
+        out_ref[...] = total_ref[...].astype(out_ref.dtype)
+
+
+def expert_of(rows, gate_weight, up_weight, down_weight):
+    count, width = rows.shape
+    units = gate_weight.shape[1]
+    tile = UNITS if units % UNITS == 0 else units
+    return pl.pallas_call(
+        expert_kernel,
+        grid=(units // tile,),
+        out_shape=jax.ShapeDtypeStruct((count, width), jnp.bfloat16),
+        in_specs=[
+            pl.BlockSpec((count, width), lambda step: (0, 0)),
+            pl.BlockSpec((width, tile), lambda step: (0, step)),
+            pl.BlockSpec((width, tile), lambda step: (0, step)),
+            pl.BlockSpec((tile, width), lambda step: (step, 0)),
+        ],
+        out_specs=pl.BlockSpec((count, width), lambda step: (0, 0)),
+        scratch_shapes=[pltpu.VMEM((count, width), jnp.float32)],
+        compiler_params=pltpu.CompilerParams(vmem_limit_bytes=48 * 1024 * 1024),
+        name="experts",
+        cost_estimate=pl.CostEstimate(
+            flops=6 * count * width * units,
+            bytes_accessed=6 * width * units + 4 * count * width,
+            transcendentals=count * units,
+        ),
+    )(rows, gate_weight, up_weight, down_weight)
 
 
 def shards(
@@ -211,13 +285,14 @@
     packed = lanes // head_size
     sends = pack_heads(queries[0], keys[0], values[0], sp_size, chunks, lanes)
     arrived_qkv = [
-        lax.all_to_all(send, "sp", split_axis=0, concat_axis=0, tiled=True) for send in sends
+        lax.all_to_all(send, SEQ, split_axis=0, concat_axis=0, tiled=True) for send in sends
     ]
-    weight_shards = gather_shards(out_weight, "dp")
+    weight_shards = gather_start(out_weight, "dp")
     gains = jnp.stack([jnp.tile(query_gain, packed), jnp.tile(key_gain, packed)])
     level = forget_cache[0]
     level_columns = level.T
     returned_heads = []
+    blocks = []
     for chunk in range(chunks):
         first = chunk * packed
         block = attend(
@@ -228,15 +303,17 @@
             tokens,
             head_size,
         )
+        blocks.append(block)
         returned_heads.append(
             lax.all_to_all(
                 block.reshape(sp_size, tokens, lanes),
-                "sp",
+                SEQ,
                 split_axis=0,
                 concat_axis=0,
                 tiled=True,
             )
         )
+    weight_shards = gather_rest(weight_shards, "dp", blocks)
     token_attn = (
         jnp.stack(returned_heads, axis=1)
         .transpose(2, 0, 1, 3)
@@ -274,12 +351,7 @@
         tiled=True,
     )
     flat_rows = arrived.reshape(-1, width)
-    gate = jnp.dot(flat_rows, expert_gate[0], preferred_element_type=jnp.float32)
-    upper = jnp.dot(flat_rows, expert_up[0], preferred_element_type=jnp.float32)
-    hidden = (jax.nn.silu(gate) * upper).astype(jnp.bfloat16)
-    result = jnp.dot(hidden, expert_down[0], preferred_element_type=jnp.float32).astype(
-        jnp.bfloat16
-    )
+    result = expert_of(flat_rows, expert_gate[0], expert_up[0], expert_down[0])
     returned = lax.all_to_all(
         result.reshape(arrived.shape), ("sp", "dp"), split_axis=0, concat_axis=0, tiled=True
     )

time: 222 us -> 216 us (0.973)
  matrix products: 24.6 us -> 11 us
  Pallas kernels: 11.8 us -> 23.9 us
  waiting for transfers between devices: 101 us -> 97.7 us
    ppermute x3, waiting for transfers between devices: 22.8 us -> 0.01 us  [the longest x2 0.01 us: gather_rest(): lax.ppermute(part, axis, xor_pairs(size, stride))]
    all_to_all x4, waiting for transfers between devices: 30.3 us -> 49.4 us  [the longest x2 33.2 us: shards(): lax.all_to_all(send, SEQ, split_axis=0, concat_axis=0, tiled=True)]
    dot_general x2 -> x0, matrix products: 13.6 us -> none  [the longest x1 9.91 us: shards(): jnp.dot(hidden, expert_down[0], preferred_element_type=jnp.float32)]
    pallas_call x0 -> x2, Pallas kernels: none -> 12.2 us  [the longest x1 12.2 us: expert_of(): pl.pallas_call(expert_kernel, grid=(units // tile,), out_shape=jax.ShapeD...]
where the time goes in v2:
time: 216 us; the launch traced here: 215 us
  waiting for transfers between devices  97.7 us (45%)
  blocking collectives  52.1 us (24%)
  Pallas kernels  23.9 us (11%)
  starting transfers between devices  23.7 us (11%)
  matrix products  11 us (5%)
  local copies, waits for them, and re-layouts  5.05 us (2%)
    all_to_all x1, blocking collectives, shards(): lax.all_to_all(send.reshape(experts, capacity, width), ('sp', 'dp'), spli...  52.1 us
    all_to_all x1, waiting for transfers between devices, shards(): lax.all_to_all(result.reshape(arrived.shape), ('sp', 'dp'), split_axis=0,...  48.3 us
    all_to_all x2, waiting for transfers between devices, shards(): lax.all_to_all(send, SEQ, split_axis=0, concat_axis=0, tiled=True)  33.2 us
    all_to_all x2, waiting for transfers between devices, shards(): lax.all_to_all(block.reshape(sp_size, tokens, lanes), SEQ, split_axis=0,...  16.2 us
    pallas_call x1, Pallas kernels, expert_of(): pl.pallas_call(expert_kernel, grid=(units // tile,), out_shape=jax.ShapeD...  12.2 us
    all_to_all x2, starting transfers between devices, shards(): lax.all_to_all(send, SEQ, split_axis=0, concat_axis=0, tiled=True)  11 us
    pallas_call x2, Pallas kernels, attend(): pl.pallas_call(functools.partial(attend_kernel, tokens, head_size, rows),...  8.99 us
    dot_general x4, matrix products, shards(): jnp.dot(token_attn, shard, preferred_element_type=jnp.float32)  8.35 us
  transfers between devices with their start and end apart: 8, of which 5 were waited for; matrix products, arithmetic and copies ran while one was open for 5% of the time, Pallas kernels for 4%

profile of v2, /device:TPU:0, one launch (start us, length us, event | category | flops | bytes accessed | tf_op | source)
XLA Modules:
  0.0 215.0 jit_solution(7602604140313151991)
XLA Ops:
  0.0 2.8 %pack_heads.1 = (bf16[8,384,128]{2,1,0:T(8,128)(2,1)}, bf16[8,384,128]{2,1,0:T(8,128)(2,1)}) custom-call(bf16[128,2048]{1,0:T(8,128)(2,1)} %bitcast.86, bf16[128,2048]{1,0:T(8,128)(2,1)} %bitcast.87, bf16[128,2048]{1,0:T(8,128)(2,1)} %bitcast.88), custom_call_target="tpu_custom_call" | custom-call | flops 262144 | bytes 3145728 | tf_op jit(solution)/shard_map/pack_heads/pallas_call | solution.py:41
  2.8 7.4 %all-to-all-start = ((bf16[8,384,128]{2,1,0:T(8,128)(2,1)}), bf16[8,384,128]{2,1,0:T(8,128)(2,1)S(1)}, u32[]{:S(2)}, u32[]{:S(2)}) async-start(bf16[8,384,128]{2,1,0:T(8,128)(2,1)} %get-tuple-element.7), calls=%async_computation | async-start | bytes 1572864 | tf_op jit(solution)/shard_map/all_to_all | solution.py:288
  10.2 1.5 collective-permute-start
  11.7 18.7 %all-to-all-done.qkv_ref = bf16[8,384,128]{2,1,0:T(8,128)(2,1)S(1)} async-done(((bf16[8,384,128]{2,1,0:T(8,128)(2,1)}), bf16[8,384,128]{2,1,0:T(8,128)(2,1)S(1)}, u32[]{:S(2)}, u32[]{:S(2)}) %all-to-all-start) | async-done | bytes 786464 | tf_op jit(solution)/shard_map/all_to_all | solution.py:288
  30.3 3.6 %all-to-all-start.2 = ((bf16[8,384,128]{2,1,0:T(8,128)(2,1)}), bf16[8,384,128]{2,1,0:T(8,128)(2,1)S(1)}, u32[]{:S(2)}, u32[]{:S(2)}) async-start(bf16[8,384,128]{2,1,0:T(8,128)(2,1)} %get-tuple-element.8), calls=%async_computation.2 | async-start | bytes 1572864 | tf_op jit(solution)/shard_map/all_to_all | solution.py:288
  34.0 0.2 copy.33
  34.4 0.2 fusion.20
  34.6 4.5 %attend.2 = bf16[1024,128]{1,0:T(8,128)(2,1)S(1)} custom-call(bf16[8,384,128]{2,1,0:T(8,128)(2,1)S(1)} %all-to-all-done.qkv_ref, f32[2,128]{1,0:T(2,128)S(1)} %pad_maximum_fusion.1.gains_ref, f32[2,1024]{1,0:T(2,128)S(1)} %get-tuple-element.19.level_ref, f32[1024,2]{1,0:T(8,128)S(1)} %get-tuple-element.17.column_ref), custom_call_target="tpu_custom_call" | custom-call | flops 1073741824 | bytes 1048576 | tf_op jit(solution)/shard_map/attend/pallas_call | solution.py:141
  39.1 0.6 slice.58.refs_1_
  39.7 14.6 %all-to-all-done.2.qkv_ref = bf16[8,384,128]{2,1,0:T(8,128)(2,1)S(1)} async-done(((bf16[8,384,128]{2,1,0:T(8,128)(2,1)}), bf16[8,384,128]{2,1,0:T(8,128)(2,1)S(1)}, u32[]{:S(2)}, u32[]{:S(2)}) %all-to-all-start.2) | async-done | bytes 786464 | tf_op jit(solution)/shard_map/all_to_all | solution.py:288
  54.3 4.5 %attend.3 = bf16[1024,128]{1,0:T(8,128)(2,1)S(1)} custom-call(bf16[8,384,128]{2,1,0:T(8,128)(2,1)S(1)} %all-to-all-done.2.qkv_ref, f32[2,128]{1,0:T(2,128)S(1)} %pad_maximum_fusion.1.gains_ref, f32[2,1024]{1,0:T(2,128)S(1)} %get-tuple-element.20.level_ref, f32[1024,2]{1,0:T(8,128)S(1)} %get-tuple-element.18.column_ref), custom_call_target="tpu_custom_call" | custom-call | flops 1073741824 | bytes 1048576 | tf_op jit(solution)/shard_map/attend/pallas_call | solution.py:141
  58.8 0.6 slice.59.refs_2_
  59.4 0.9 copy.35
  60.3 3.9 %all-to-all-start.3 = ((bf16[8,128,128]{1,2,0:T(8,128)(2,1)}), bf16[8,128,128]{1,2,0:T(8,128)(2,1)S(1)}, u32[]{:S(2)}, u32[]{:S(2)}) async-start(bf16[8,128,128]{1,2,0:T(8,128)(2,1)} %copy.35), calls=%async_computation.3 | async-start | bytes 524288 | tf_op jit(solution)/shard_map/all_to_all | solution.py:308
  64.6 0.6 reduce-window.6
  65.4 0.9 copy.34
  66.3 7.5 %all-to-all-done.3 = bf16[8,128,128]{1,2,0:T(8,128)(2,1)S(1)} async-done(((bf16[8,128,128]{1,2,0:T(8,128)(2,1)}), bf16[8,128,128]{1,2,0:T(8,128)(2,1)S(1)}, u32[]{:S(2)}, u32[]{:S(2)}) %all-to-all-start.3) | async-done | bytes 262176 | tf_op jit(solution)/shard_map/all_to_all | solution.py:308
  73.7 3.6 %all-to-all-start.1 = ((bf16[8,128,128]{1,2,0:T(8,128)(2,1)}), bf16[8,128,128]{1,2,0:T(8,128)(2,1)S(1)}, u32[]{:S(2)}, u32[]{:S(2)}) async-start(bf16[8,128,128]{1,2,0:T(8,128)(2,1)} %copy.34), calls=%async_computation.1 | async-start | bytes 524288 | tf_op jit(solution)/shard_map/all_to_all | solution.py:308
  77.7 8.7 %all-to-all-done.1 = bf16[8,128,128]{1,2,0:T(8,128)(2,1)S(1)} async-done(((bf16[8,128,128]{1,2,0:T(8,128)(2,1)}), bf16[8,128,128]{1,2,0:T(8,128)(2,1)S(1)}, u32[]{:S(2)}, u32[]{:S(2)}) %all-to-all-start.1) | async-done | bytes 262176 | tf_op jit(solution)/shard_map/all_to_all | solution.py:308
  86.5 2.1 fusion.23
  88.6 2.1 fusion.21
  90.7 2.1 fusion.22
  92.7 2.2 %broadcast_select_fusion.7 = (f32[128,512]{1,0:T(8,128)S(1)}, f32[128,512]{1,0:T(8,128)S(1)}, f32[128,512]{1,0:T(8,128)S(1)}, f32[128,512]{1,0:T(8,128)S(1)}) fusion(pred[]{:T(512)S(6)} %ne.6, f32[128,512]{1,0:T(8,128)S(1)} %fusion.21, pred[]{:T(512)S(6)} %ne.7, f32[128,512]{1,0:T(8,128)S(1)} %fusion.22, f32[128,512]{1,0:T(8,128)S(1)} %fusion.23, ...), kind=kOutput, calls=%fused_computation.30 | convolution fusion | flops 268959744 | bytes 4456450 | tf_op jit(solution)/shard_map/dot_general | solution.py:323
  94.9 0.2 fusion.4
  95.2 0.4 copy-done.2
  95.6 0.8 convolution_convert_fusion
  96.4 52.1 %all_to_all.30 = bf16[32,16,2048]{2,1,0:T(8,128)(2,1)S(1)} all-to-all(bf16[32,16,2048]{2,1,0:T(8,128)(2,1)S(1)} %bitcast.82), channel_id=1, replica_groups=mesh['sp'=8,'dp'=4] {'sp','dp'}, dimensions={0} | all-to-all | bytes 4194304 | tf_op jit(solution)/shard_map/all_to_all | solution.py:346
  148.5 12.2 %experts.1 = bf16[512,2048]{1,0:T(8,128)(2,1)} custom-call(bf16[512,2048]{1,0:T(8,128)(2,1)S(1)} %bitcast.73, bf16[2048,1024]{1,0:T(8,128)(2,1)} %bitcast.90, bf16[2048,1024]{1,0:T(8,128)(2,1)} %bitcast.91, bf16[1024,2048]{1,0:T(8,128)(2,1)} %bitcast.92), custom_call_target="tpu_custom_call" | custom-call | flops 6442450944 | bytes 16777216 | tf_op jit(solution)/shard_map/experts/pallas_call | solution.py:238
  160.7 3.7 %all-to-all-start.5 = ((bf16[32,16,2048]{2,1,0:T(8,128)(2,1)}), bf16[32,16,2048]{2,1,0:T(8,128)(2,1)S(1)}, u32[]{:S(2)}, u32[]{:S(2)}) async-start(bf16[32,16,2048]{2,1,0:T(8,128)(2,1)} %bitcast.27), calls=%async_computation.5 | async-start | bytes 4194304 | tf_op jit(solution)/shard_map/all_to_all | solution.py:355
  164.8 48.3 %all-to-all-done.5 = bf16[32,16,2048]{2,1,0:T(8,128)(2,1)S(1)} async-done(((bf16[32,16,2048]{2,1,0:T(8,128)(2,1)}), bf16[32,16,2048]{2,1,0:T(8,128)(2,1)S(1)}, u32[]{:S(2)}, u32[]{:S(2)}) %all-to-all-start.5) | async-done | bytes 2097184 | tf_op jit(solution)/shard_map/all_to_all | solution.py:355
  213.1 0.5 convolution_multiply_fusion.1
  213.6 1.4 fusion.3
  (47 shorter events, 1.7 us)
Async XLA Ops:
  0.0 34.0 %copy-start.1 = (f32[1,4,1024]{2,1,0:T(4,128)S(1)}, f32[1,4,1024]{2,1,0:T(4,128)}, u32[]{:S(2)}) copy-start(f32[1,4,1024]{2,1,0:T(4,128)} %param.19) | copy-start | bytes 49156
  2.8 31.5 %copy-start.6 = (f32[64]{0:T(128)S(1)}, f32[64]{0:T(128)}, u32[]{:S(2)}) copy-start(f32[64]{0:T(128)} %param.20) | copy-start | bytes 772
  2.8 31.6 %copy-start.7 = (f32[64]{0:T(128)S(1)}, f32[64]{0:T(128)}, u32[]{:S(2)}) copy-start(f32[64]{0:T(128)} %param.21) | copy-start | bytes 772
  2.8 27.6 %all-to-all-start = ((bf16[8,384,128]{2,1,0:T(8,128)(2,1)}), bf16[8,384,128]{2,1,0:T(8,128)(2,1)S(1)}, u32[]{:S(2)}, u32[]{:S(2)}) async-start(bf16[8,384,128]{2,1,0:T(8,128)(2,1)} %get-tuple-element.7), calls=%async_computation | async-start | bytes 1572864 | tf_op jit(solution)/shard_map/all_to_all | solution.py:288
  10.2 49.2 %collective-permute-start = (bf16[2048,512]{1,0:T(8,128)(2,1)}, bf16[2048,512]{1,0:T(8,128)(2,1)}, u32[]{:S(2)}, u32[]{:S(2)}) collective-permute-start(bf16[2048,512]{1,0:T(8,128)(2,1)} %param.22), channel_id=1, source_target_pairs={{0,2},{1,3},{2,0},{3,1},{4,6},{5,7},{6,4},{7,5},{8,10},{9,11},{10,... | collective-permute-start | bytes 6291464 | tf_op jit(solution)/shard_map/ppermute | solution.py:182
  30.3 24.0 %all-to-all-start.2 = ((bf16[8,384,128]{2,1,0:T(8,128)(2,1)}), bf16[8,384,128]{2,1,0:T(8,128)(2,1)S(1)}, u32[]{:S(2)}, u32[]{:S(2)}) async-start(bf16[8,384,128]{2,1,0:T(8,128)(2,1)} %get-tuple-element.8), calls=%async_computation.2 | async-start | bytes 1572864 | tf_op jit(solution)/shard_map/all_to_all | solution.py:288
  33.9 56.7 %collective-permute-start.2 = (bf16[2048,512]{1,0:T(8,128)(2,1)}, bf16[2048,512]{1,0:T(8,128)(2,1)}, u32[]{:S(2)}, u32[]{:S(2)}) collective-permute-start(bf16[2048,512]{1,0:T(8,128)(2,1)} %param.22), channel_id=1, source_target_pairs={{0,1},{1,0},{2,3},{3,2},{4,5},{5,4},{6,7},{7,6},{8,9},{9,8},{10,11... | collective-permute-start | bytes 6291464 | tf_op jit(solution)/shard_map/ppermute | solution.py:191
  59.4 4.8 %copy-start.4 = (s32[1,128,2]{1,2,0:T(2,128)S(1)}, s32[1,128,2]{1,2,0:T(2,128)}, u32[]{:S(2)}) copy-start(s32[1,128,2]{1,2,0:T(2,128)} %param.24) | copy-start | bytes 3076
  59.4 33.3 %collective-permute-start.1 = (bf16[2048,512]{1,0:T(8,128)(2,1)}, bf16[2048,512]{1,0:T(8,128)(2,1)}, u32[]{:S(2)}, u32[]{:S(2)}) collective-permute-start(bf16[2048,512]{1,0:T(8,128)(2,1)} %tie.1), channel_id=1, source_target_pairs={{0,1},{1,0},{2,3},{3,2},{4,5},{5,4},{6,7},{7,6},{8,9},{9,8},{10,11... | collective-permute-start | bytes 6291464 | tf_op jit(solution)/shard_map/ppermute | solution.py:191
  60.3 13.5 %all-to-all-start.3 = ((bf16[8,128,128]{1,2,0:T(8,128)(2,1)}), bf16[8,128,128]{1,2,0:T(8,128)(2,1)S(1)}, u32[]{:S(2)}, u32[]{:S(2)}) async-start(bf16[8,128,128]{1,2,0:T(8,128)(2,1)} %copy.35), calls=%async_computation.3 | async-start | bytes 524288 | tf_op jit(solution)/shard_map/all_to_all | solution.py:308
  73.7 12.7 %all-to-all-start.1 = ((bf16[8,128,128]{1,2,0:T(8,128)(2,1)}), bf16[8,128,128]{1,2,0:T(8,128)(2,1)S(1)}, u32[]{:S(2)}, u32[]{:S(2)}) async-start(bf16[8,128,128]{1,2,0:T(8,128)(2,1)} %copy.34), calls=%async_computation.1 | async-start | bytes 524288 | tf_op jit(solution)/shard_map/all_to_all | solution.py:308
  92.7 2.2 %copy-start = (bf16[1,128,2048]{2,1,0:T(8,128)(2,1)S(1)}, bf16[1,128,2048]{2,1,0:T(8,128)(2,1)}, u32[]{:S(2)}) copy-start(bf16[1,128,2048]{2,1,0:T(8,128)(2,1)} %param.15) | copy-start | bytes 1572868
  94.9 0.7 copy-start.2
  160.7 3.8 %copy-start.3 = (f32[1,128,2]{1,2,0:T(2,128)S(1)}, f32[1,128,2]{1,2,0:T(2,128)}, u32[]{:S(2)}) copy-start(f32[1,128,2]{1,2,0:T(2,128)} %param.26) | copy-start | bytes 3076
  160.7 4.0 %copy-start.5 = (f32[1,128]{1,0:T(1,128)S(1)}, f32[1,128]{1,0:T(1,128)}, u32[]{:S(2)}) copy-start(f32[1,128]{1,0:T(1,128)} %param.25) | copy-start | bytes 1540
  160.7 52.4 %all-to-all-start.5 = ((bf16[32,16,2048]{2,1,0:T(8,128)(2,1)}), bf16[32,16,2048]{2,1,0:T(8,128)(2,1)S(1)}, u32[]{:S(2)}, u32[]{:S(2)}) async-start(bf16[32,16,2048]{2,1,0:T(8,128)(2,1)} %bitcast.27), calls=%async_computation.5 | async-start | bytes 4194304 | tf_op jit(solution)/shard_map/all_to_all | solution.py:355
